TPU v7x, 512 devices: a whole 4x8x8 slice. The times are simulated.
512 devices in a mesh: ep: 32 (over z, x), tp: 16 (over y, core).
Axes of the slice: x: 4, y: 8, z: 8, core: 2. Of those that a mesh axis runs over, the one named last changes fastest.
Arguments:
- blender_incoming_features: bfloat16 [8192, 4096], P('ep', 'tp'), may hold values from -6 to 6
- entry_latent_matrix: bfloat16 [8192, 2048], P('ep', 'tp'), may hold values from -6 to 6
- exit_latent_matrix: bfloat16 [8192, 2048], P('ep', 'tp'), may hold values from -6 to 6
- unactivated_valve: bfloat16 [8192, 4096], P('ep', 'tp'), may hold values from -6 to 6
- presoftplus_strides: float32 [8192, 64], P('ep', 'tp'), may hold values from -7 to 7
- extra_attenuation: float32 [8192, 64], P('ep', 'tp'), may hold values from -1 to 0
- incoming_feature_kernel: bfloat16 [4, 4096], P(None, 'tp'), may hold values from -3 to 3
- entry_latent_kernel: bfloat16 [4, 2048], P(None, 'tp'), may hold values from -3 to 3
- exit_latent_kernel: bfloat16 [4, 2048], P(None, 'tp'), may hold values from -3 to 3
- stride_offset_vector: float32 [64], P('tp'), may hold values from -1 to 1
- attenuation_speed_exponent: float32 [64], P('tp'), may hold values from -16 to -3
- bypass_coef_vector: float32 [64], P('tp'), may hold values from 0.5 to 4
- cluster_rescale_coefs: bfloat16 [4096], P('tp'), may hold values from 0.099609375 to 1.8984375
- blender_result_matrix: bfloat16 [4096, 2048], P('tp'), may hold values from -0.09375 to 0.09375
- latter_microbatch_activations: bfloat16 [8192, 2048], P('ep'), may hold values from -6 to 6
- specialist_rescale_coefs: bfloat16 [2048], replicated, may hold values from 0.099609375 to 1.8984375
- specialist_valve_matrix: bfloat16 [32, 2048, 4096], P('ep', None, 'tp'), may hold values from -0.125 to 0.125
- specialist_expand_matrix: bfloat16 [32, 2048, 4096], P('ep', None, 'tp'), may hold values from -0.125 to 0.125
- specialist_contract_matrix: bfloat16 [32, 4096, 2048], P('ep', 'tp'), may hold values from -0.125 to 0.125
- specialist_picks: int32 [8192, 2], P('ep'), may hold values from 0 to 31, all different within a row; in each aligned block of 256 rows (0 to 255, 256 to 511, ...) at most 24 rows name the same one
- selected_specialist_coefs: float32 [8192, 2], P('ep'), may hold values from 0.1 to 1
Outputs:
- mixed_a: bfloat16 [8192, 2048], P(('ep', 'tp'))
- mixed_b: bfloat16 [8192, 2048], P('ep', 'tp')
Inputs may be any that keep to these rules, and one draw needn't show every extreme that they name: `specialist_picks`: in each aligned block of 256 rows, the rows of one index of ep, no expert is named by more than 24 rows, a bound that some block reaches.
All inputs are finite; a program needn't handle non-finite values.
Results may differ from a plain program's by a relative error of at most 0.019.
Values may be sent and summed in bfloat16 or wider, within the bound.
No kernel may reach another device: no remote copies, remote signals or barrier semaphores. Data moves between devices by JAX's collectives and lax.ppermute only.
A program may use at most 64 MiB of HBM per device.

v0:
```python
import jax
import jax.numpy as jnp
from jax import lax
from jax.sharding import Mesh
from jax.sharding import PartitionSpec as P

HEADS = 64
HEAD_DIM = 64
SHARING_CLUSTERS = 16
STATE = 128
BLOCK = 64
TOPK = 2
EP = ("ep_0", "ep_1")
TP = ("tp_0", "tp_1")
EP_TP = ("ep_0", "ep_1", "tp_0", "tp_1")
NORM_EPS = 1e-06


def from_behind(block, axis, distance):
    devices = range(lax.axis_size(axis))
    route = [(i - distance, i) for i in devices if i - distance in devices]
    return lax.ppermute(block, axis, route)


def filled_with(x, identity):
    return jax.tree.map(
        lambda part, zero: jnp.zeros_like(part) + jnp.asarray(zero, part.dtype), x, identity
    )


def carried_in(x, axes, combine, identity):
    before = start = filled_with(x, identity)
    running = x
    for axis in reversed(axes):
        count, place = (lax.axis_size(axis), lax.axis_index(axis))
        pieces = jax.tree.map(
            lambda part, kind: lax.all_gather(part.astype(kind), axis),
            running,
            (jnp.bfloat16, jnp.bfloat16),
        )
        inside, running = (start, start)
        for k in range(count):
            passed = k < place
            running = combine(
                running, jax.tree.map(lambda part, own: part[k].astype(own.dtype), pieces, x)
            )
            inside = jax.tree.map(lambda new, old: jnp.where(passed, new, old), running, inside)
        before = combine(inside, before)
    return before


def in_blocks(x, dim, count):
    before, after = (x.shape[:dim], x.shape[dim + 1 :])
    return jnp.moveaxis(x.reshape(*before, count, -1, *after), dim, 0)


def summed_on_arrival(x, axis, dim):
    tiles = in_blocks(x, dim, lax.axis_size(axis))
    arrived = lax.all_to_all(tiles, axis, split_axis=0, concat_axis=0, tiled=True)
    return arrived.astype(jnp.float32).sum(axis=0)


def summed_rows(x, axes, dim):
    for axis in axes:
        x = lax.psum_scatter(x, axis, scatter_dimension=dim, tiled=True)
    return x


def conv_silu(inputs, rim_rows, weight):
    tap_count = weight.shape[0]
    context_span = inputs.shape[0]
    joined = jnp.concatenate([rim_rows, inputs], axis=0).astype(jnp.float32)
    kernel = weight.astype(jnp.float32)
    running_total = kernel[0] * joined[0:context_span]
    for offset in range(1, tap_count):
        running_total = running_total + kernel[offset] * joined[offset : offset + context_span]
    return jax.nn.silu(running_total)


def block_step(carry_state, inputs):
    scaled_x, b_block, c_block, log_block = inputs
    context_span = log_block.shape[0]
    running = jnp.cumsum(log_block, axis=0)
    causal = (jnp.arange(context_span)[:, None] >= jnp.arange(context_span)[None, :])[
        :, :, None, None
    ]
    log_gap = running[:, None] - running[None, :]
    weights = jnp.where(causal, jnp.exp(jnp.where(causal, log_gap, 0.0)), 0.0)
    scores = jnp.einsum("lgn,sgn->lsg", c_block, b_block, preferred_element_type=jnp.float32)
    inside = jnp.einsum("lsgj,sgjp->lgjp", scores[..., None] * weights, scaled_x)
    c_wide = c_block.astype(jnp.float32)
    b_wide = b_block.astype(jnp.float32)
    before = jnp.einsum("lgn,gjpn->lgjp", c_wide, carry_state) * jnp.exp(running)[..., None]
    to_end = jnp.exp(running[-1] - running)
    carry_state = carry_state * jnp.exp(running[-1])[..., None, None] + jnp.einsum(
        "sgn,sgjp->gjpn", b_wide, scaled_x * to_end[..., None]
    )
    return (carry_state, inside + before)


def combine_states(earlier, later):
    early_state, early_log = earlier
    late_state, late_log = later
    return (early_state * jnp.exp(late_log)[..., None, None] + late_state, early_log + late_log)


def local(
    blender_incoming_features,
    entry_latent_matrix,
    exit_latent_matrix,
    unactivated_valve,
    presoftplus_strides,
    extra_attenuation,
    incoming_feature_kernel,
    entry_latent_kernel,
    exit_latent_kernel,
    stride_offset_vector,
    attenuation_speed_exponent,
    bypass_coef_vector,
    cluster_rescale_coefs,
    blender_result_matrix,
    latter_microbatch_activations,
    specialist_rescale_coefs,
    specialist_valve_matrix,
    specialist_expand_matrix,
    specialist_contract_matrix,
    specialist_picks,
    selected_specialist_coefs,
):
    tap_count = incoming_feature_kernel.shape[0]
    tok_rows = blender_incoming_features.shape[0]
    groups_local = entry_latent_matrix.shape[1] // STATE
    members_within_cluster = HEADS // SHARING_CLUSTERS
    tail_start = tok_rows - tap_count + 1
    rim_x, rim_b, rim_c = from_behind(
        (
            blender_incoming_features[tail_start:],
            entry_latent_matrix[tail_start:],
            exit_latent_matrix[tail_start:],
        ),
        EP,
        1,
    )
    conv_x_out = conv_silu(blender_incoming_features, rim_x, incoming_feature_kernel).reshape(
        tok_rows, groups_local, members_within_cluster, HEAD_DIM
    )
    conv_b_out = (
        conv_silu(entry_latent_matrix, rim_b, entry_latent_kernel)
        .astype(jnp.bfloat16)
        .reshape(tok_rows, groups_local, STATE)
    )
    conv_c_out = (
        conv_silu(exit_latent_matrix, rim_c, exit_latent_kernel)
        .astype(jnp.bfloat16)
        .reshape(tok_rows, groups_local, STATE)
    )
    stride_amount = jax.nn.softplus(presoftplus_strides + stride_offset_vector[None, :])
    attenuation_exponent = (
        -jnp.exp(attenuation_speed_exponent)[None, :] * stride_amount + extra_attenuation
    ).reshape(tok_rows, groups_local, members_within_cluster)
    scaled_x = (
        conv_x_out
        * stride_amount.reshape(tok_rows, groups_local, members_within_cluster)[..., None]
    )
    blocks = tok_rows // BLOCK

    def as_blocks(array_value):
        return array_value.reshape((blocks, BLOCK) + array_value.shape[1:])

    start_state = jnp.zeros((groups_local, members_within_cluster, HEAD_DIM, STATE), jnp.float32)
    end_state, block_out = lax.scan(
        block_step,
        start_state,
        (
            as_blocks(scaled_x),
            as_blocks(conv_b_out),
            as_blocks(conv_c_out),
            as_blocks(attenuation_exponent),
        ),
    )
    running = jnp.cumsum(attenuation_exponent, axis=0)
    enter_state = carried_in(
        (end_state, running[-1]),
        EP,
        combine_states,
        (jnp.zeros_like(end_state), jnp.zeros_like(running[-1])),
    )[0]
    carried = (
        jnp.einsum("lgn,gjpn->lgjp", conv_c_out.astype(jnp.float32), enter_state)
        * jnp.exp(running)[..., None]
    )
    ssd_out = (
        block_out.reshape(tok_rows, groups_local, members_within_cluster, HEAD_DIM)
        + carried
        + bypass_coef_vector.reshape(groups_local, members_within_cluster)[None, :, :, None]
        * conv_x_out
    )
    gated_out = ssd_out.reshape(tok_rows, -1) * jax.nn.silu(unactivated_valve.astype(jnp.float32))
    grouped = gated_out.reshape(tok_rows, groups_local, -1)
    grouped = grouped * lax.rsqrt(jnp.mean(grouped * grouped, axis=-1, keepdims=True) + NORM_EPS)
    normed = (grouped.reshape(tok_rows, -1) * cluster_rescale_coefs.astype(jnp.float32)).astype(
        jnp.bfloat16
    )
    mixed_a = summed_on_arrival(
        jnp.dot(normed, blender_result_matrix, preferred_element_type=jnp.float32).astype(
            jnp.bfloat16
        ),
        TP,
        0,
    ).astype(jnp.bfloat16)
    ep_count = lax.axis_size(EP)
    token_count = latter_microbatch_activations.shape[0]
    model_width = latter_microbatch_activations.shape[1]
    local_experts = specialist_valve_matrix.shape[0]
    expert_count = ep_count * local_experts
    capacity = 3 * token_count * TOPK // (2 * expert_count)
    slot_total = expert_count * capacity
    widened = latter_microbatch_activations.astype(jnp.float32)
    normed_b = (
        widened
        * lax.rsqrt(jnp.mean(widened * widened, axis=-1, keepdims=True) + NORM_EPS)
        * specialist_rescale_coefs.astype(jnp.float32)
    ).astype(jnp.bfloat16)
    flat_routes = specialist_picks.reshape(-1)
    assigned = flat_routes.shape[0]
    positions = jnp.arange(assigned, dtype=jnp.int32)
    earlier_same = (flat_routes[:, None] == flat_routes[None, :]) & (
        positions[None, :] < positions[:, None]
    )
    slot_rank = jnp.sum(earlier_same.astype(jnp.int32), axis=1)
    slot_of = flat_routes * capacity + slot_rank
    slot_ids = jnp.arange(slot_total, dtype=jnp.int32)
    placing = (slot_ids[:, None] == slot_of[None, :]).astype(jnp.bfloat16)
    placing = jnp.sum(placing.reshape(slot_total, token_count, TOPK), axis=2)
    outgoing = jnp.dot(placing, normed_b, preferred_element_type=jnp.float32).astype(jnp.bfloat16)
    outgoing = outgoing.reshape(ep_count, local_experts, capacity, model_width)
    slice_width = model_width // lax.axis_size(TP)
    my_columns = lax.dynamic_slice_in_dim(
        outgoing, lax.axis_index(TP) * slice_width, slice_width, 3
    )
    arrived = lax.all_to_all(my_columns, EP, split_axis=0, concat_axis=0, tiled=True)
    gathered_piece = lax.all_gather(arrived, TP, axis=3, tiled=True)
    gate_sum = jnp.einsum(
        "sejd,edf->sejf",
        gathered_piece,
        specialist_valve_matrix,
        preferred_element_type=jnp.float32,
    )
    up_sum = jnp.einsum(
        "sejd,edf->sejf",
        gathered_piece,
        specialist_expand_matrix,
        preferred_element_type=jnp.float32,
    )
    hidden = (jax.nn.silu(gate_sum) * up_sum).astype(jnp.bfloat16)
    partial_out = jnp.einsum(
        "sejf,efd->sejd", hidden, specialist_contract_matrix, preferred_element_type=jnp.float32
    )
    summed = (
        summed_rows(partial_out.astype(jnp.bfloat16), TP, 3)
        .astype(jnp.float32)
        .astype(jnp.bfloat16)
    )
    returned = lax.all_to_all(summed, EP, split_axis=0, concat_axis=0, tiled=True)
    returned = returned.reshape(slot_total, -1)
    token_slots = slot_of.reshape(token_count, TOPK)
    combined = jnp.zeros((token_count, returned.shape[1]), jnp.float32)
    for pick_index in range(TOPK):
        selecting = (token_slots[:, pick_index][:, None] == slot_ids[None, :]).astype(jnp.bfloat16)
        chosen_rows = jnp.dot(selecting, returned, preferred_element_type=jnp.float32)
        combined = combined + chosen_rows * selected_specialist_coefs[:, pick_index][:, None]
    mixed_b = combined.astype(jnp.bfloat16)
    return (mixed_a, mixed_b)


def solution(mesh):
    split = Mesh(mesh.devices.reshape(8, 4, 8, 2), ("ep_0", "ep_1", "tp_0", "tp_1"))
    in_specs = (
        P(EP, TP),
        P(EP, TP),
        P(EP, TP),
        P(EP, TP),
        P(EP, TP),
        P(EP, TP),
        P(None, TP),
        P(None, TP),
        P(None, TP),
        P(TP),
        P(TP),
        P(TP),
        P(TP),
        P(TP, None),
        P(EP, None),
        P(),
        P(EP, None, TP),
        P(EP, None, TP),
        P(EP, TP, None),
        P(EP, None),
        P(EP, None),
    )
    out_specs = (P(EP_TP, None), P(EP, TP))
    return jax.shard_map(local, mesh=split, in_specs=in_specs, out_specs=out_specs, check_vma=False)
```

profile of v0, /device:TPU:8, one launch (start us, length us, event | category | flops | bytes accessed | tf_op | source)
XLA Modules:
  0.0 217.6 jit_solution(4881775239269224496)
XLA Ops:
  7.2 0.9 copy.135
  10.5 1.5 fusion.40
  12.1 2.5 %convolution_convert_fusion.1 = bf16[768,2048]{1,0:T(8,128)(2,1)S(1)} fusion(bf16[768,256]{1,0:T(8,128)(2,1)S(1)} %fusion.71, bf16[256,2048]{1,0:T(8,128)(2,1)} %param.37, f32[2048]{0:T(1024)S(1)} %convert_element_type.381, f32[256]{0:T(256)S(1)} %add_rsqrt_fusion), kind=kOutput, calls=%fused_computation.46 | convolution fusion | flops 808976384 | bytes 4596736 | tf_op jit(solution)/shard_map/dot_general | solution.py:235
  14.7 24.7 %all_to_all.15 = bf16[32,1,24,128]{3,2,1,0:T(8,128)(2,1)} all-to-all(bf16[32,1,24,128]{3,2,1,0:T(8,128)(2,1)S(1)} %constant_dynamic-slice_fusion.2), channel_id=1, replica_groups=mesh['ep_0'=8,'ep_1'=4,'tp_0'=8,'tp_1'=2] {'ep_0','ep_1'}, dimensions={0} | all-to-all | bytes 393216 | tf_op jit(solution)/shard_map/all_to_all | solution.py:241
  39.5 1.9 collective-permute-start
  41.4 3.4 %collective-permute-start.2 = (bf16[3,128]{1,0:T(4,128)(2,1)S(1)}, bf16[3,128]{1,0:T(4,128)(2,1)S(1)}, u32[]{:S(2)}, u32[]{:S(2)}) collective-permute-start(bf16[3,128]{1,0:T(4,128)(2,1)S(1)} %slice.198), channel_id=1, source_target_pairs={{0,16},{16,32},{32,48},{48,64},{64,80},{80,96},{96,112},{112,128},... | collective-permute-start | bytes 2312 | tf_op jit(solution)/shard_map/ppermute | solution.py:22
  44.9 1.2 reduce-window.6
  46.8 3.3 %collective-permute-start.1 = (bf16[3,128]{1,0:T(4,128)(2,1)S(1)}, bf16[3,128]{1,0:T(4,128)(2,1)S(1)}, u32[]{:S(2)}, u32[]{:S(2)}) collective-permute-start(bf16[3,128]{1,0:T(4,128)(2,1)S(1)} %slice.189), channel_id=1, source_target_pairs={{0,16},{16,32},{32,48},{48,64},{64,80},{80,96},{96,112},{112,128},... | collective-permute-start | bytes 2312 | tf_op jit(solution)/shard_map/ppermute | solution.py:22
  50.0 9.3 %all_gather.21 = bf16[4,1,4]{2,1,0:T(2,128)(2,1)S(1)} all-gather(bf16[1,1,4]{2,1,0:T(2,128)(2,1)S(1)} %slice.260), channel_id=1, replica_groups=mesh['ep_0'=8,'ep_1'=4,'tp_0'=8,'tp_1'=2] {'ep_1'}, dimensions={0}, use_global_device_ids=true | all-gather | bytes 40 | tf_op jit(solution)/shard_map/all_gather | solution.py:37
  59.4 13.9 %all_gather.22 = bf16[8,1,4]{2,1,0:T(2,128)(2,1)S(1)} all-gather(bf16[1,1,4]{2,1,0:T(2,128)(2,1)S(1)} %get-tuple-element.133), channel_id=1, replica_groups=mesh['ep_0'=8,'ep_1'=4,'tp_0'=8,'tp_1'=2] {'ep_0'}, dimensions={0}, use_global_device_ids=true | all-gather | bytes 72 | tf_op jit(solution)/shard_map/all_gather | solution.py:37
  74.9 6.9 %all-gather.3.cloned.1.call-done = bf16[32,1,24,2048]{3,2,0,1:T(8,128)(2,1)} async-done(((bf16[32,1,24,128]{3,2,0,1:T(8,128)(2,1)}), bf16[32,1,24,2048]{3,2,0,1:T(8,128)(2,1)}) %all-gather.3.cloned.1.call-update) | async-done | bytes 3145744 | tf_op jit(solution)/shard_map/all_gather | solution.py:242
  81.8 4.1 %fusion.44 = f32[32,1,24,256]{3,2,0,1:T(8,128)} fusion(bf16[32,1,24,2048]{3,2,0,1:T(8,128)(2,1)} %all-gather.3.cloned.1.call-done, bf16[1,2048,256]{2,1,0:T(8,128)(2,1)} %param.39), kind=kOutput, calls=%fused_computation.60 | convolution fusion | flops 805306368 | bytes 4980736 | tf_op jit(solution)/shard_map/sejd,edf->sejf/dot_general | solution.py:243
  85.8 7.5 %fusion.39 = bf16[32,1,24,2048]{3,2,0,1:T(8,128)(2,1)} fusion(bf16[1,256,2048]{2,1,0:T(8,128)(2,1)S(1)} %copy-done, bf16[32,1,24,2048]{3,2,0,1:T(8,128)(2,1)} %all-gather.3.cloned.1.call-done, bf16[1,2048,256]{2,1,0:T(8,128)(2,1)} %param.40, f32[32,1,24,256]{3,2,0,1:T(8,128)} %fusion.44), kind=kOutput, calls=%fused_computation.51 | convolution fusion | flops 1613365248 | bytes 9175040 | tf_op jit(solution)/shard_map/sejf,efd->sejd/dot_general | solution.py:256
  93.3 1.0 copy-done.1
  94.3 16.0 %while.13 = (s32[]{:T(128)}, f32[1,4,64,128]{3,2,1,0:T(8,128)S(1)}, f32[4,64,1,4,64]{1,0,4,3,2:T(4,128)S(1)}, f32[4,64,1,4]{3,1,2,0:T(8,128)S(1)}, f32[4,64,1,4,...) while((s32[]{:T(128)}, f32[1,4,64,128]{3,2,1,0:T(8,128)S(1)}, ...), condition=%wide.region_2.3_spmd.clone, body=%wide.region_0.2_spmd.clone.sunk | while | flops 11800579 | bytes 1400524 | solution.py:171
  95.3 2.8 %dynamic_update_slice.6 = f32[4,64,1,4,64]{1,0,4,3,2:T(4,128)S(1)} dynamic-update-slice(f32[4,64,1,4,64]{1,0,4,3,2:T(4,128)S(1)} %get-tuple-element.209, f32[1,64,1,4,64]{1,0,4,3,2:T(1,128)S(1)} %bitcast.305, s32[]{:T(128)} %get-tuple-element.207, s32[]{:T(128)} %constant.33.clone.1..sunk, s32[]{:T(128)} %constant.33.clone.1..sunk, s32[]{:T(128)} %constant.33.clone.1..sunk, s32[]{:T(128)} %constant.33.clone.1..sunk) | dynamic-update-slice | bytes 131076 | tf_op jit(solution)/shard_map/while/body/jit(dynamic_update_index_in_dim)/dynamic_update_slice | solution.py:171
  99.3 2.8 %dynamic_update_slice.6 = f32[4,64,1,4,64]{1,0,4,3,2:T(4,128)S(1)} dynamic-update-slice(f32[4,64,1,4,64]{1,0,4,3,2:T(4,128)S(1)} %get-tuple-element.209, f32[1,64,1,4,64]{1,0,4,3,2:T(1,128)S(1)} %bitcast.305, s32[]{:T(128)} %get-tuple-element.207, s32[]{:T(128)} %constant.33.clone.1..sunk, s32[]{:T(128)} %constant.33.clone.1..sunk, s32[]{:T(128)} %constant.33.clone.1..sunk, s32[]{:T(128)} %constant.33.clone.1..sunk) | dynamic-update-slice | bytes 131076 | tf_op jit(solution)/shard_map/while/body/jit(dynamic_update_index_in_dim)/dynamic_update_slice | solution.py:171
  103.3 2.8 %dynamic_update_slice.6 = f32[4,64,1,4,64]{1,0,4,3,2:T(4,128)S(1)} dynamic-update-slice(f32[4,64,1,4,64]{1,0,4,3,2:T(4,128)S(1)} %get-tuple-element.209, f32[1,64,1,4,64]{1,0,4,3,2:T(1,128)S(1)} %bitcast.305, s32[]{:T(128)} %get-tuple-element.207, s32[]{:T(128)} %constant.33.clone.1..sunk, s32[]{:T(128)} %constant.33.clone.1..sunk, s32[]{:T(128)} %constant.33.clone.1..sunk, s32[]{:T(128)} %constant.33.clone.1..sunk) | dynamic-update-slice | bytes 131076 | tf_op jit(solution)/shard_map/while/body/jit(dynamic_update_index_in_dim)/dynamic_update_slice | solution.py:171
  107.3 2.8 %dynamic_update_slice.6 = f32[4,64,1,4,64]{1,0,4,3,2:T(4,128)S(1)} dynamic-update-slice(f32[4,64,1,4,64]{1,0,4,3,2:T(4,128)S(1)} %get-tuple-element.209, f32[1,64,1,4,64]{1,0,4,3,2:T(1,128)S(1)} %bitcast.305, s32[]{:T(128)} %get-tuple-element.207, s32[]{:T(128)} %constant.33.clone.1..sunk, s32[]{:T(128)} %constant.33.clone.1..sunk, s32[]{:T(128)} %constant.33.clone.1..sunk, s32[]{:T(128)} %constant.33.clone.1..sunk) | dynamic-update-slice | bytes 131076 | tf_op jit(solution)/shard_map/while/body/jit(dynamic_update_index_in_dim)/dynamic_update_slice | solution.py:171
  110.8 12.6 %all-gather = bf16[4,4,64,128]{3,2,1,0:T(8,128)(2,1)S(1)} all-gather(bf16[1,4,64,128]{3,2,1,0:T(8,128)(2,1)S(1)} %convert_element_type.353), channel_id=2, replica_groups=mesh['ep_0'=8,'ep_1'=4,'tp_0'=8,'tp_1'=2] {'ep_1'}, dimensions={0}, use_global_device_ids=true | all-gather | bytes 327680 | tf_op jit(solution)/shard_map/all_gather | solution.py:37
  123.6 27.3 %all_gather.25 = bf16[8,1,4,64,128]{4,3,2,1,0:T(8,128)(2,1)S(1)} all-gather(bf16[1,1,4,64,128]{4,3,2,1,0:T(8,128)(2,1)S(1)} %fusion.134), channel_id=1, replica_groups=mesh['ep_0'=8,'ep_1'=4,'tp_0'=8,'tp_1'=2] {'ep_0'}, dimensions={0}, use_global_device_ids=true | all-gather | bytes 589824 | tf_op jit(solution)/shard_map/all_gather | solution.py:37
  151.6 2.7 %convolution_convert_fusion.2 = bf16[256,2048]{1,0:T(8,128)(2,1)} fusion(bf16[256,2048]{1,0:T(8,128)(2,1)} %param.36, f32[256]{0:T(256)S(1)} %convert_element_type.375, f32[256]{0:T(256)S(1)} %add_rsqrt_fusion.1, f32[256,256]{1,0:T(8,128)S(1)} %copy.134, bf16[256,256]{1,0:T(8,128)(2,1)S(1)} %copy-done.3), kind=kOutput, calls=%fused_computation.54 | convolution fusion | flops 269549568 | bytes 2492416 | tf_op jit(solution)/shard_map/dot_general | solution.py:205
  154.3 5.4 %all-to-all-start = ((bf16[16,16,2048]{2,1,0:T(8,128)(2,1)}), bf16[16,16,2048]{2,1,0:T(8,128)(2,1)}, u32[]{:S(2)}, u32[]{:S(2)}) async-start(bf16[16,16,2048]{2,1,0:T(8,128)(2,1)} %bitcast.49), calls=%async_computation | async-start | bytes 2097152 | tf_op jit(solution)/shard_map/all_to_all | solution.py:59
  159.9 3.8 %copy.143 = bf16[32,1,24,256]{2,0,1,3:T(8,128)(2,1)S(1)} copy(bf16[32,1,24,256]{3,2,0,1:T(8,128)(2,1)} %reduce-scatter.5.cloned.1.call-done) | data formatting | bytes 786432
  163.7 4.2 %reshape.641 = bf16[256,768]{1,0:T(8,128)(2,1)} reshape(bf16[256,1,32,24]{3,2,1,0:T(8,128)(2,1)S(1)} %bitcast.307) | data formatting | bytes 786432
  168.0 15.1 %reduce-scatter.7.cloned.1.call-done = bf16[128,768]{1,0:T(8,128)(2,1)} async-done(((bf16[256,768]{1,0:T(8,128)(2,1)}), bf16[128,768]{1,0:T(8,128)(2,1)}) %reduce-scatter.7.cloned.1.call-update) | async-done | bytes 196624
  183.1 2.6 %reshape.642 = bf16[128,1,32,24]{3,2,1,0:T(8,128)(2,1)S(1)} reshape(bf16[128,768]{1,0:T(8,128)(2,1)} %reduce-scatter.7.cloned.1.call-done) | data formatting | bytes 393216
  185.7 1.7 copy.144
  187.5 10.2 %all-to-all-start.2 = ((bf16[32,1,24,128]{3,2,1,0:T(8,128)(2,1)}), bf16[32,1,24,128]{3,2,1,0:T(8,128)(2,1)S(1)}, u32[]{:S(2)}, u32[]{:S(2)}) async-start(bf16[32,1,24,128]{3,2,1,0:T(8,128)(2,1)} %bitcast.73), calls=%async_computation.3 | async-start | bytes 393216 | tf_op jit(solution)/shard_map/all_to_all | solution.py:264
  197.7 2.0 reduce_sum.54
  199.7 10.1 %all-to-all-done.2 = bf16[32,1,24,128]{3,2,1,0:T(8,128)(2,1)S(1)} async-done(((bf16[32,1,24,128]{3,2,1,0:T(8,128)(2,1)}), bf16[32,1,24,128]{3,2,1,0:T(8,128)(2,1)S(1)}, u32[]{:S(2)}, u32[]{:S(2)}) %all-to-all-start.2) | async-done | bytes 196640 | tf_op jit(solution)/shard_map/all_to_all | solution.py:264
  210.2 0.9 fusion.63
  (153 shorter events, 11.1 us)
Async XLA Ops:
  7.2 78.7 %copy-start = (bf16[1,256,2048]{2,1,0:T(8,128)(2,1)S(1)}, bf16[1,256,2048]{2,1,0:T(8,128)(2,1)}, u32[]{:S(2)}) copy-start(bf16[1,256,2048]{2,1,0:T(8,128)(2,1)} %param.41) | copy-start | bytes 3145732
  7.2 74.6 %all-gather.3.cloned.1.call-start = ((), (), s32[]{:S(2)}) async-start(), calls=%async_computation.5 | async-start | bytes 3342336 | tf_op jit(solution)/shard_map/all_gather | solution.py:242
  12.0 27.5 %copy-start.2 = (bf16[256,256]{1,0:T(8,128)(2,1)S(1)}, bf16[256,256]{1,0:T(8,128)(2,1)}, u32[]{:S(2)}) copy-start(bf16[256,256]{1,0:T(8,128)(2,1)} %param.23) | copy-start | bytes 393220
  12.0 29.3 %copy-start.4 = (bf16[256,128]{1,0:T(8,128)(2,1)S(1)}, bf16[256,128]{1,0:T(8,128)(2,1)}, u32[]{:S(2)}) copy-start(bf16[256,128]{1,0:T(8,128)(2,1)} %param.25) | copy-start | bytes 196612
  12.0 32.7 %copy-start.13 = (f32[4]{0:T(128)S(1)}, f32[4]{0:T(128)}, u32[]{:S(2)}) copy-start(f32[4]{0:T(128)} %param.33) | copy-start | bytes 52
  12.0 32.7 %copy-start.7 = (f32[256,4]{0,1:T(4,128)S(1)}, f32[256,4]{0,1:T(4,128)}, u32[]{:S(2)}) copy-start(f32[256,4]{0,1:T(4,128)} %param.28) | copy-start | bytes 12292
  12.0 32.7 %copy-start.8 = (f32[256,4]{0,1:T(4,128)S(1)}, f32[256,4]{0,1:T(4,128)}, u32[]{:S(2)}) copy-start(f32[256,4]{0,1:T(4,128)} %param.27) | copy-start | bytes 12292
  12.1 32.7 %copy-start.12 = (f32[4]{0:T(128)S(1)}, f32[4]{0:T(128)}, u32[]{:S(2)}) copy-start(f32[4]{0:T(128)} %param.32) | copy-start | bytes 52
  12.1 34.3 %copy-start.5 = (bf16[256,128]{1,0:T(8,128)(2,1)S(1)}, bf16[256,128]{1,0:T(8,128)(2,1)}, u32[]{:S(2)}) copy-start(bf16[256,128]{1,0:T(8,128)(2,1)} %param.24) | copy-start | bytes 196612
  12.1 61.4 %copy-start.10 = (bf16[4,128]{1,0:T(4,128)(2,1)S(1)}, bf16[4,128]{1,0:T(4,128)(2,1)}, u32[]{:S(2)}) copy-start(bf16[4,128]{1,0:T(4,128)(2,1)} %param.31) | copy-start | bytes 3076
  12.1 61.4 %copy-start.11 = (bf16[4,128]{1,0:T(4,128)(2,1)S(1)}, bf16[4,128]{1,0:T(4,128)(2,1)}, u32[]{:S(2)}) copy-start(bf16[4,128]{1,0:T(4,128)(2,1)} %param.30) | copy-start | bytes 3076
  12.1 61.4 %copy-start.6 = (bf16[4,256]{1,0:T(4,128)(2,1)S(1)}, bf16[4,256]{1,0:T(4,128)(2,1)}, u32[]{:S(2)}) copy-start(bf16[4,256]{1,0:T(4,128)(2,1)} %param.29) | copy-start | bytes 6148
  12.1 61.7 %copy-start.14 = (bf16[256]{0:T(256)(128)(2,1)S(1)}, bf16[256]{0:T(256)(128)(2,1)}, u32[]{:S(2)}) copy-start(bf16[256]{0:T(256)(128)(2,1)} %param.35) | copy-start | bytes 1540
  39.4 120.5 %reduce-scatter.5.cloned.1.call-start = ((), (), s32[]{:S(2)}) async-start(), calls=%async_computation.6 | async-start | bytes 3538944 | tf_op jit(solution)/shard_map/reduce_scatter | solution.py:65
  39.5 34.6 %collective-permute-start = (bf16[3,256]{1,0:T(4,128)(2,1)S(1)}, bf16[3,256]{1,0:T(4,128)(2,1)S(1)}, u32[]{:S(2)}, u32[]{:S(2)}) collective-permute-start(bf16[3,256]{1,0:T(4,128)(2,1)S(1)} %slice.180), channel_id=1, source_target_pairs={{0,16},{16,32},{32,48},{48,64},{64,80},{80,96},{96,112},{112,128},... | collective-permute-start | bytes 4616 | tf_op jit(solution)/shard_map/ppermute | solution.py:22
  41.4 32.4 %collective-permute-start.2 = (bf16[3,128]{1,0:T(4,128)(2,1)S(1)}, bf16[3,128]{1,0:T(4,128)(2,1)S(1)}, u32[]{:S(2)}, u32[]{:S(2)}) collective-permute-start(bf16[3,128]{1,0:T(4,128)(2,1)S(1)} %slice.198), channel_id=1, source_target_pairs={{0,16},{16,32},{32,48},{48,64},{64,80},{80,96},{96,112},{112,128},... | collective-permute-start | bytes 2312 | tf_op jit(solution)/shard_map/ppermute | solution.py:22
  46.8 27.1 %collective-permute-start.1 = (bf16[3,128]{1,0:T(4,128)(2,1)S(1)}, bf16[3,128]{1,0:T(4,128)(2,1)S(1)}, u32[]{:S(2)}, u32[]{:S(2)}) collective-permute-start(bf16[3,128]{1,0:T(4,128)(2,1)S(1)} %slice.189), channel_id=1, source_target_pairs={{0,16},{16,32},{32,48},{48,64},{64,80},{80,96},{96,112},{112,128},... | collective-permute-start | bytes 2312 | tf_op jit(solution)/shard_map/ppermute | solution.py:22
  93.3 1.0 copy-start.1
  94.3 56.5 %copy-start.15 = (f32[4]{0:T(128)S(1)}, f32[4]{0:T(128)}, u32[]{:S(2)}) copy-start(f32[4]{0:T(128)} %param.34) | copy-start | bytes 52
  110.3 41.1 %copy-start.3 = (bf16[256,256]{1,0:T(8,128)(2,1)S(1)}, bf16[256,256]{1,0:T(8,128)(2,1)}, u32[]{:S(2)}) copy-start(bf16[256,256]{1,0:T(8,128)(2,1)} %param.26) | copy-start | bytes 393220
  154.3 33.2 %all-to-all-start = ((bf16[16,16,2048]{2,1,0:T(8,128)(2,1)}), bf16[16,16,2048]{2,1,0:T(8,128)(2,1)}, u32[]{:S(2)}, u32[]{:S(2)}) async-start(bf16[16,16,2048]{2,1,0:T(8,128)(2,1)} %bitcast.49), calls=%async_computation | async-start | bytes 2097152 | tf_op jit(solution)/shard_map/all_to_all | solution.py:59
  159.7 23.4 %reduce-scatter.7.cloned.1.call-start = ((), (), s32[]{:S(2)}) async-start(), calls=%async_computation.7 | async-start | bytes 589824
  163.7 34.0 %copy-start.9 = (f32[256,2]{0,1:T(2,128)S(1)}, f32[256,2]{0,1:T(2,128)}, u32[]{:S(2)}) copy-start(f32[256,2]{0,1:T(2,128)} %param.43) | copy-start | bytes 6148
  187.5 22.3 %all-to-all-start.2 = ((bf16[32,1,24,128]{3,2,1,0:T(8,128)(2,1)}), bf16[32,1,24,128]{3,2,1,0:T(8,128)(2,1)S(1)}, u32[]{:S(2)}, u32[]{:S(2)}) async-start(bf16[32,1,24,128]{3,2,1,0:T(8,128)(2,1)} %bitcast.73), calls=%async_computation.3 | async-start | bytes 393216 | tf_op jit(solution)/shard_map/all_to_all | solution.py:264
Sparse Core Ops, SparseCore 0:
  39.5 42.2 all-gather.2
  93.4 48.1 reduce-scatter.4
  168.1 14.9 reduce-scatter.6
where the time goes:
time: 218 us
  blocking collectives  87.9 us (40%)
  waiting for transfers between devices  32.2 us (15%)
  local copies, waits for them, and re-layouts  28.7 us (13%)
  starting transfers between devices  24.4 us (11%)
  matrix products  21 us (10%)
  between operations  14.4 us (7%)
  other arithmetic  8.82 us (4%)
    all_gather x4, blocking collectives, carried_in(): lax.all_gather(part.astype(kind), axis)  63.2 us
    all_to_all x1, blocking collectives, local(): lax.all_to_all(my_columns, EP, split_axis=0, concat_axis=0, tiled=True)  24.7 us
    unnamed x4, waiting for transfers between devices  15.2 us
    unnamed x37, local copies, waits for them, and re-layouts  14.4 us
    dynamic_update_slice x4, local copies, waits for them, and re-layouts, local(): lax.scan(block_step, start_state, (as_blocks(scaled_x), as_blocks(conv_b_...  11.2 us
    all_to_all x1, starting transfers between devices, local(): lax.all_to_all(summed, EP, split_axis=0, concat_axis=0, tiled=True)  10.2 us
    all_to_all x1, waiting for transfers between devices, local(): lax.all_to_all(summed, EP, split_axis=0, concat_axis=0, tiled=True)  10.1 us
    ppermute x3, starting transfers between devices, from_behind(): return lax.ppermute(block, axis, route)  8.48 us
  transfers between devices with their start and end apart: 8, of which 3 were waited for; matrix products, arithmetic and copies ran while one was open for 17% of the time, Pallas kernels for 0%

commit v1 on v0

--- a/solution.py
+++ b/solution.py
@@ -14,6 +14,11 @@
 TP = ("tp_0", "tp_1")
 EP_TP = ("ep_0", "ep_1", "tp_0", "tp_1")
 NORM_EPS = 1e-06
+
+
+def all_by_exchange(x, axis, d):
+    stack = jnp.stack([x] * lax.axis_size(axis))
+    return jnp.concatenate(lax.all_to_all(stack, axis, 0, 0), axis=d)
 
 
 def from_behind(block, axis, distance):
@@ -239,7 +244,7 @@
         outgoing, lax.axis_index(TP) * slice_width, slice_width, 3
     )
     arrived = lax.all_to_all(my_columns, EP, split_axis=0, concat_axis=0, tiled=True)
-    gathered_piece = lax.all_gather(arrived, TP, axis=3, tiled=True)
+    gathered_piece = all_by_exchange(arrived, TP, 3)
     gate_sum = jnp.einsum(
         "sejd,edf->sejf",
         gathered_piece,

time: 218 us -> 262 us (1.20)
  waiting for transfers between devices: 32.2 us -> 56.5 us
  local copies, waits for them, and re-layouts: 28.7 us -> 44.1 us
  starting transfers between devices: 24.4 us -> 32.9 us
    all_to_all x0 -> x1, waiting for transfers between devices: none -> 34.1 us  [all_by_exchange(): return jnp.concatenate(lax.all_to_all(stack, axis, 0, 0), axis=d)]
    another operation x3 -> x5, local copies, waits for them, and re-layouts: 0.15 us -> 8.23 us
    all_to_all x0 -> x1, starting transfers between devices: none -> 7.71 us  [all_by_exchange(): return jnp.concatenate(lax.all_to_all(stack, axis, 0, 0), axis=d)]
    reshape x1 -> x2, local copies, waits for them, and re-layouts: 0.01 us -> 7.21 us  [the longest x1 7.2 us: all_by_exchange(): return jnp.concatenate(lax.all_to_all(stack, axis, 0, 0), axis=d)]
    all_gather x1 -> x0, waiting for transfers between devices: 6.89 us -> none  [local(): gathered_piece = lax.all_gather(arrived, TP, axis=3, tiled=True)]
    unnamed x4 -> x3, waiting for transfers between devices: 15.2 us -> 11.6 us
    unnamed x37 -> x39, local copies, waits for them, and re-layouts: 14.4 us -> 14.4 us
  transfers between devices with their start and end apart: 8 -> 8, of which waited for: 3 -> 4; matrix products, arithmetic and copies ran while one was open for 17% -> 14% of each run, Pallas kernels for 0% -> 0%
where the time goes in v1:
time: 262 us; the launch traced here: 261 us
  blocking collectives  85.7 us (33%)
  waiting for transfers between devices  56.5 us (22%)
  local copies, waits for them, and re-layouts  44.1 us (17%)
  starting transfers between devices  32.9 us (13%)
  matrix products  18.5 us (7%)
  between operations  14.7 us (6%)
  other arithmetic  8.82 us (3%)
    all_gather x4, blocking collectives, carried_in(): lax.all_gather(part.astype(kind), axis)  61.1 us
    all_to_all x1, waiting for transfers between devices, all_by_exchange(): return jnp.concatenate(lax.all_to_all(stack, axis, 0, 0), axis=d)  34.1 us
    all_to_all x1, blocking collectives, local(): lax.all_to_all(my_columns, EP, split_axis=0, concat_axis=0, tiled=True)  24.6 us
    unnamed x39, local copies, waits for them, and re-layouts  14.4 us
    unnamed x3, waiting for transfers between devices  11.6 us
    dynamic_update_slice x4, local copies, waits for them, and re-layouts, local(): lax.scan(block_step, start_state, (as_blocks(scaled_x), as_blocks(conv_b_...  11.2 us
    all_to_all x1, waiting for transfers between devices, local(): lax.all_to_all(summed, EP, split_axis=0, concat_axis=0, tiled=True)  10.1 us
    all_to_all x1, starting transfers between devices, local(): lax.all_to_all(summed, EP, split_axis=0, concat_axis=0, tiled=True)  9.58 us
  transfers between devices with their start and end apart: 8, of which 4 were waited for; matrix products, arithmetic and copies ran while one was open for 14% of the time, Pallas kernels for 0%

profile of v1, /device:TPU:8, one launch (start us, length us, event | category | flops | bytes accessed | tf_op | source)
XLA Modules:
  0.0 261.4 jit_solution(4554807395674338553)
XLA Ops:
  10.4 1.5 fusion.36
  12.0 2.3 convolution_convert_fusion.1
  14.4 24.6 %all_to_all.23 = bf16[32,1,24,128]{3,2,1,0:T(8,128)(2,1)S(1)} all-to-all(bf16[32,1,24,128]{3,2,1,0:T(8,128)(2,1)S(1)} %constant_dynamic-slice_fusion.2), channel_id=1, replica_groups=mesh['ep_0'=8,'ep_1'=4,'tp_0'=8,'tp_1'=2] {'ep_0','ep_1'}, dimensions={0} | all-to-all | bytes 393216 | tf_op jit(solution)/shard_map/all_to_all | solution.py:246
  39.0 2.3 stack.2
  41.4 7.7 %all-to-all-start.2 = ((bf16[16,32,1,24,128]{4,3,1,2,0:T(8,128)(2,1)}), bf16[16,32,1,24,128]{4,3,1,2,0:T(8,128)(2,1)}, u32[]{:S(2)}, u32[]{:S(2)}) async-start(bf16[16,32,1,24,128]{4,3,1,2,0:T(8,128)(2,1)} %stack.2), calls=%async_computation.2 | async-start | bytes 6291456 | tf_op jit(solution)/shard_map/all_to_all | solution.py:21
  49.1 1.9 collective-permute-start
  51.0 3.4 %collective-permute-start.2 = (bf16[3,128]{1,0:T(4,128)(2,1)S(1)}, bf16[3,128]{1,0:T(4,128)(2,1)S(1)}, u32[]{:S(2)}, u32[]{:S(2)}) collective-permute-start(bf16[3,128]{1,0:T(4,128)(2,1)S(1)} %slice.198), channel_id=1, source_target_pairs={{0,16},{16,32},{32,48},{48,64},{64,80},{80,96},{96,112},{112,128},... | collective-permute-start | bytes 2312 | tf_op jit(solution)/shard_map/ppermute | solution.py:27
  56.4 3.3 %collective-permute-start.1 = (bf16[3,128]{1,0:T(4,128)(2,1)S(1)}, bf16[3,128]{1,0:T(4,128)(2,1)S(1)}, u32[]{:S(2)}, u32[]{:S(2)}) collective-permute-start(bf16[3,128]{1,0:T(4,128)(2,1)S(1)} %slice.189), channel_id=1, source_target_pairs={{0,16},{16,32},{32,48},{48,64},{64,80},{80,96},{96,112},{112,128},... | collective-permute-start | bytes 2312 | tf_op jit(solution)/shard_map/ppermute | solution.py:27
  59.7 9.3 %all_gather.18 = bf16[4,1,4]{2,1,0:T(2,128)(2,1)S(1)} all-gather(bf16[1,1,4]{2,1,0:T(2,128)(2,1)S(1)} %slice.260), channel_id=1, replica_groups=mesh['ep_0'=8,'ep_1'=4,'tp_0'=8,'tp_1'=2] {'ep_1'}, dimensions={0}, use_global_device_ids=true | all-gather | bytes 40 | tf_op jit(solution)/shard_map/all_gather | solution.py:42
  69.0 14.1 %all_gather.19 = bf16[8,1,4]{2,1,0:T(2,128)(2,1)S(1)} all-gather(bf16[1,1,4]{2,1,0:T(2,128)(2,1)S(1)} %get-tuple-element.133), channel_id=1, replica_groups=mesh['ep_0'=8,'ep_1'=4,'tp_0'=8,'tp_1'=2] {'ep_0'}, dimensions={0}, use_global_device_ids=true | all-gather | bytes 72 | tf_op jit(solution)/shard_map/all_gather | solution.py:42
  84.7 34.1 %all-to-all-done.2 = bf16[16,32,1,24,128]{4,3,1,2,0:T(8,128)(2,1)} async-done(((bf16[16,32,1,24,128]{4,3,1,2,0:T(8,128)(2,1)}), bf16[16,32,1,24,128]{4,3,1,2,0:T(8,128)(2,1)}, u32[]{:S(2)}, u32[]{:S(2)}) %all-to-all-start.2) | async-done | bytes 3145760 | tf_op jit(solution)/shard_map/all_to_all | solution.py:21
  118.9 7.2 %copy.138 = bf16[32,1,24,16,128]{4,3,2,0,1:T(8,128)(2,1)} copy(bf16[32,1,24,16,128]{4,2,0,1,3:T(8,128)(2,1)} %bitcast.54) | data formatting | bytes 6291456 | tf_op jit(solution)/shard_map/reshape | solution.py:21
  126.1 5.8 %reshape.623 = bf16[32,24,2048]{2,1,0:T(8,128)(2,1)} reshape(bf16[32,1,24,16,128]{4,3,2,0,1:T(8,128)(2,1)} %copy.138) | data formatting | bytes 6291456 | tf_op jit(solution)/shard_map/reshape.63
  131.9 3.1 %convolution_bitcast_fusion.5 = f32[32,1,24,256]{3,2,0,1:T(8,128)S(1)} fusion(bf16[32,24,2048]{2,1,0:T(8,128)(2,1)} %reshape.623, bf16[1,2048,256]{2,1,0:T(8,128)(2,1)} %param.39), kind=kOutput, calls=%fused_computation.57 | convolution fusion | flops 805306368 | bytes 4980736 | tf_op jit(solution)/shard_map/sejd,edf->sejf/dot_general | solution.py:248
  135.0 7.2 %fusion.35 = bf16[32,1,24,2048]{3,2,0,1:T(8,128)(2,1)} fusion(bf16[1,256,2048]{2,1,0:T(8,128)(2,1)S(1)} %copy-done, bf16[32,24,2048]{2,1,0:T(8,128)(2,1)} %reshape.623, bf16[1,2048,256]{2,1,0:T(8,128)(2,1)} %param.40, f32[32,1,24,256]{3,2,0,1:T(8,128)S(1)} %convolution_bitcast_fusion.5), kind=kOutput, calls=%fused_computation.47 | convolution fusion | flops 1613365248 | bytes 9175040 | tf_op jit(solution)/shard_map/sejf,efd->sejd/dot_general | solution.py:261
  143.3 15.9 %while.13 = (s32[]{:T(128)}, f32[1,4,64,128]{3,2,1,0:T(8,128)S(1)}, f32[4,64,1,4,64]{1,0,4,3,2:T(4,128)S(1)}, f32[4,64,1,4]{3,1,2,0:T(8,128)S(1)}, f32[4,64,1,4,...) while((s32[]{:T(128)}, f32[1,4,64,128]{3,2,1,0:T(8,128)S(1)}, ...), condition=%wide.region_2.3_spmd.clone, body=%wide.region_0.2_spmd.clone.sunk | while | flops 11800579 | bytes 1400524 | solution.py:176
  144.3 2.8 %dynamic_update_slice.6 = f32[4,64,1,4,64]{1,0,4,3,2:T(4,128)S(1)} dynamic-update-slice(f32[4,64,1,4,64]{1,0,4,3,2:T(4,128)S(1)} %get-tuple-element.209, f32[1,64,1,4,64]{1,0,4,3,2:T(1,128)S(1)} %bitcast.295, s32[]{:T(128)} %get-tuple-element.207, s32[]{:T(128)} %constant.33.clone.1..sunk, s32[]{:T(128)} %constant.33.clone.1..sunk, s32[]{:T(128)} %constant.33.clone.1..sunk, s32[]{:T(128)} %constant.33.clone.1..sunk) | dynamic-update-slice | bytes 131076 | tf_op jit(solution)/shard_map/while/body/jit(dynamic_update_index_in_dim)/dynamic_update_slice | solution.py:176
  148.3 2.8 %dynamic_update_slice.6 = f32[4,64,1,4,64]{1,0,4,3,2:T(4,128)S(1)} dynamic-update-slice(f32[4,64,1,4,64]{1,0,4,3,2:T(4,128)S(1)} %get-tuple-element.209, f32[1,64,1,4,64]{1,0,4,3,2:T(1,128)S(1)} %bitcast.295, s32[]{:T(128)} %get-tuple-element.207, s32[]{:T(128)} %constant.33.clone.1..sunk, s32[]{:T(128)} %constant.33.clone.1..sunk, s32[]{:T(128)} %constant.33.clone.1..sunk, s32[]{:T(128)} %constant.33.clone.1..sunk) | dynamic-update-slice | bytes 131076 | tf_op jit(solution)/shard_map/while/body/jit(dynamic_update_index_in_dim)/dynamic_update_slice | solution.py:176
  152.3 2.8 %dynamic_update_slice.6 = f32[4,64,1,4,64]{1,0,4,3,2:T(4,128)S(1)} dynamic-update-slice(f32[4,64,1,4,64]{1,0,4,3,2:T(4,128)S(1)} %get-tuple-element.209, f32[1,64,1,4,64]{1,0,4,3,2:T(1,128)S(1)} %bitcast.295, s32[]{:T(128)} %get-tuple-element.207, s32[]{:T(128)} %constant.33.clone.1..sunk, s32[]{:T(128)} %constant.33.clone.1..sunk, s32[]{:T(128)} %constant.33.clone.1..sunk, s32[]{:T(128)} %constant.33.clone.1..sunk) | dynamic-update-slice | bytes 131076 | tf_op jit(solution)/shard_map/while/body/jit(dynamic_update_index_in_dim)/dynamic_update_slice | solution.py:176
  156.3 2.8 %dynamic_update_slice.6 = f32[4,64,1,4,64]{1,0,4,3,2:T(4,128)S(1)} dynamic-update-slice(f32[4,64,1,4,64]{1,0,4,3,2:T(4,128)S(1)} %get-tuple-element.209, f32[1,64,1,4,64]{1,0,4,3,2:T(1,128)S(1)} %bitcast.295, s32[]{:T(128)} %get-tuple-element.207, s32[]{:T(128)} %constant.33.clone.1..sunk, s32[]{:T(128)} %constant.33.clone.1..sunk, s32[]{:T(128)} %constant.33.clone.1..sunk, s32[]{:T(128)} %constant.33.clone.1..sunk) | dynamic-update-slice | bytes 131076 | tf_op jit(solution)/shard_map/while/body/jit(dynamic_update_index_in_dim)/dynamic_update_slice | solution.py:176
  159.8 12.4 %all-gather = bf16[4,4,64,128]{3,2,1,0:T(8,128)(2,1)S(1)} all-gather(bf16[1,4,64,128]{3,2,1,0:T(8,128)(2,1)S(1)} %convert_element_type.353), channel_id=2, replica_groups=mesh['ep_0'=8,'ep_1'=4,'tp_0'=8,'tp_1'=2] {'ep_1'}, dimensions={0}, use_global_device_ids=true | all-gather | bytes 327680 | tf_op jit(solution)/shard_map/all_gather | solution.py:42
  172.3 25.3 %all_gather.22 = bf16[8,1,4,64,128]{4,3,2,1,0:T(8,128)(2,1)S(1)} all-gather(bf16[1,1,4,64,128]{4,3,2,1,0:T(8,128)(2,1)S(1)} %fusion.116), channel_id=1, replica_groups=mesh['ep_0'=8,'ep_1'=4,'tp_0'=8,'tp_1'=2] {'ep_0'}, dimensions={0}, use_global_device_ids=true | all-gather | bytes 589824 | tf_op jit(solution)/shard_map/all_gather | solution.py:42
  198.3 1.5 convolution_convert_fusion.2
  199.8 7.0 %all-to-all-start = ((bf16[16,16,2048]{2,1,0:T(8,128)(2,1)}), bf16[16,16,2048]{2,1,0:T(8,128)(2,1)}, u32[]{:S(2)}, u32[]{:S(2)}) async-start(bf16[16,16,2048]{2,1,0:T(8,128)(2,1)} %bitcast.49), calls=%async_computation | async-start | bytes 2097152 | tf_op jit(solution)/shard_map/all_to_all | solution.py:64
  206.9 3.8 %copy.143 = bf16[32,1,24,256]{2,0,1,3:T(8,128)(2,1)S(1)} copy(bf16[32,1,24,256]{3,2,0,1:T(8,128)(2,1)} %reduce-scatter.5.cloned.1.call-done) | data formatting | bytes 786432
  210.7 4.2 %reshape.651 = bf16[256,768]{1,0:T(8,128)(2,1)} reshape(bf16[256,1,32,24]{3,2,1,0:T(8,128)(2,1)S(1)} %bitcast.297) | data formatting | bytes 786432
  215.0 11.6 %reduce-scatter.7.cloned.1.call-done = bf16[128,768]{1,0:T(8,128)(2,1)} async-done(((bf16[256,768]{1,0:T(8,128)(2,1)}), bf16[128,768]{1,0:T(8,128)(2,1)}) %reduce-scatter.7.cloned.1.call-update) | async-done | bytes 196624
  226.6 2.6 %reshape.652 = bf16[128,1,32,24]{3,2,1,0:T(8,128)(2,1)S(1)} reshape(bf16[128,768]{1,0:T(8,128)(2,1)} %reduce-scatter.7.cloned.1.call-done) | data formatting | bytes 393216
  229.2 1.7 copy.144
  231.6 9.6 %all-to-all-start.3 = ((bf16[32,1,24,128]{3,2,1,0:T(8,128)(2,1)}), bf16[32,1,24,128]{3,2,1,0:T(8,128)(2,1)S(1)}, u32[]{:S(2)}, u32[]{:S(2)}) async-start(bf16[32,1,24,128]{3,2,1,0:T(8,128)(2,1)} %bitcast.73), calls=%async_computation.4 | async-start | bytes 393216 | tf_op jit(solution)/shard_map/all_to_all | solution.py:269
  241.2 2.0 reduce_sum.54
  243.2 10.1 %all-to-all-done.3 = bf16[32,1,24,128]{3,2,1,0:T(8,128)(2,1)S(1)} async-done(((bf16[32,1,24,128]{3,2,1,0:T(8,128)(2,1)}), bf16[32,1,24,128]{3,2,1,0:T(8,128)(2,1)S(1)}, u32[]{:S(2)}, u32[]{:S(2)}) %all-to-all-start.3) | async-done | bytes 196640 | tf_op jit(solution)/shard_map/all_to_all | solution.py:269
  (157 shorter events, 15.6 us)
Async XLA Ops:
  7.2 127.9 %copy-start = (bf16[1,256,2048]{2,1,0:T(8,128)(2,1)S(1)}, bf16[1,256,2048]{2,1,0:T(8,128)(2,1)}, u32[]{:S(2)}) copy-start(bf16[1,256,2048]{2,1,0:T(8,128)(2,1)} %param.41) | copy-start | bytes 3145732
  41.3 7.8 %copy-start.2 = (bf16[256,256]{1,0:T(8,128)(2,1)S(1)}, bf16[256,256]{1,0:T(8,128)(2,1)}, u32[]{:S(2)}) copy-start(bf16[256,256]{1,0:T(8,128)(2,1)} %param.23) | copy-start | bytes 393220
  41.3 9.7 %copy-start.4 = (bf16[256,128]{1,0:T(8,128)(2,1)S(1)}, bf16[256,128]{1,0:T(8,128)(2,1)}, u32[]{:S(2)}) copy-start(bf16[256,128]{1,0:T(8,128)(2,1)} %param.25) | copy-start | bytes 196612
  41.3 13.1 %copy-start.14 = (f32[4]{0:T(128)S(1)}, f32[4]{0:T(128)}, u32[]{:S(2)}) copy-start(f32[4]{0:T(128)} %param.33) | copy-start | bytes 52
  41.3 13.2 %copy-start.7 = (f32[256,4]{0,1:T(4,128)S(1)}, f32[256,4]{0,1:T(4,128)}, u32[]{:S(2)}) copy-start(f32[256,4]{0,1:T(4,128)} %param.28) | copy-start | bytes 12292
  41.3 13.2 %copy-start.8 = (f32[256,4]{0,1:T(4,128)S(1)}, f32[256,4]{0,1:T(4,128)}, u32[]{:S(2)}) copy-start(f32[256,4]{0,1:T(4,128)} %param.27) | copy-start | bytes 12292
  41.3 13.2 %copy-start.12 = (f32[4]{0:T(128)S(1)}, f32[4]{0:T(128)}, u32[]{:S(2)}) copy-start(f32[4]{0:T(128)} %param.32) | copy-start | bytes 52
  41.3 14.7 %copy-start.5 = (bf16[256,128]{1,0:T(8,128)(2,1)S(1)}, bf16[256,128]{1,0:T(8,128)(2,1)}, u32[]{:S(2)}) copy-start(bf16[256,128]{1,0:T(8,128)(2,1)} %param.24) | copy-start | bytes 196612
  41.3 42.0 %copy-start.10 = (bf16[4,128]{1,0:T(4,128)(2,1)S(1)}, bf16[4,128]{1,0:T(4,128)(2,1)}, u32[]{:S(2)}) copy-start(bf16[4,128]{1,0:T(4,128)(2,1)} %param.31) | copy-start | bytes 3076
  41.3 42.0 %copy-start.11 = (bf16[4,128]{1,0:T(4,128)(2,1)S(1)}, bf16[4,128]{1,0:T(4,128)(2,1)}, u32[]{:S(2)}) copy-start(bf16[4,128]{1,0:T(4,128)(2,1)} %param.30) | copy-start | bytes 3076
  41.3 42.1 %copy-start.6 = (bf16[4,256]{1,0:T(4,128)(2,1)S(1)}, bf16[4,256]{1,0:T(4,128)(2,1)}, u32[]{:S(2)}) copy-start(bf16[4,256]{1,0:T(4,128)(2,1)} %param.29) | copy-start | bytes 6148
  41.3 42.3 %copy-start.15 = (bf16[256]{0:T(256)(128)(2,1)S(1)}, bf16[256]{0:T(256)(128)(2,1)}, u32[]{:S(2)}) copy-start(bf16[256]{0:T(256)(128)(2,1)} %param.35) | copy-start | bytes 1540
  41.4 77.5 %all-to-all-start.2 = ((bf16[16,32,1,24,128]{4,3,1,2,0:T(8,128)(2,1)}), bf16[16,32,1,24,128]{4,3,1,2,0:T(8,128)(2,1)}, u32[]{:S(2)}, u32[]{:S(2)}) async-start(bf16[16,32,1,24,128]{4,3,1,2,0:T(8,128)(2,1)} %stack.2), calls=%async_computation.2 | async-start | bytes 6291456 | tf_op jit(solution)/shard_map/all_to_all | solution.py:21
  49.1 157.8 %reduce-scatter.5.cloned.1.call-start = ((), (), s32[]{:S(2)}) async-start(), calls=%async_computation.6 | async-start | bytes 3538944 | tf_op jit(solution)/shard_map/reduce_scatter | solution.py:70
  49.1 34.8 %collective-permute-start = (bf16[3,256]{1,0:T(4,128)(2,1)S(1)}, bf16[3,256]{1,0:T(4,128)(2,1)S(1)}, u32[]{:S(2)}, u32[]{:S(2)}) collective-permute-start(bf16[3,256]{1,0:T(4,128)(2,1)S(1)} %slice.180), channel_id=1, source_target_pairs={{0,16},{16,32},{32,48},{48,64},{64,80},{80,96},{96,112},{112,128},... | collective-permute-start | bytes 4616 | tf_op jit(solution)/shard_map/ppermute | solution.py:27
  51.0 32.6 %collective-permute-start.2 = (bf16[3,128]{1,0:T(4,128)(2,1)S(1)}, bf16[3,128]{1,0:T(4,128)(2,1)S(1)}, u32[]{:S(2)}, u32[]{:S(2)}) collective-permute-start(bf16[3,128]{1,0:T(4,128)(2,1)S(1)} %slice.198), channel_id=1, source_target_pairs={{0,16},{16,32},{32,48},{48,64},{64,80},{80,96},{96,112},{112,128},... | collective-permute-start | bytes 2312 | tf_op jit(solution)/shard_map/ppermute | solution.py:27
  56.4 27.3 %collective-permute-start.1 = (bf16[3,128]{1,0:T(4,128)(2,1)S(1)}, bf16[3,128]{1,0:T(4,128)(2,1)S(1)}, u32[]{:S(2)}, u32[]{:S(2)}) collective-permute-start(bf16[3,128]{1,0:T(4,128)(2,1)S(1)} %slice.189), channel_id=1, source_target_pairs={{0,16},{16,32},{32,48},{48,64},{64,80},{80,96},{96,112},{112,128},... | collective-permute-start | bytes 2312 | tf_op jit(solution)/shard_map/ppermute | solution.py:27
  142.3 1.0 copy-start.1
  143.3 54.3 %copy-start.16 = (f32[4]{0:T(128)S(1)}, f32[4]{0:T(128)}, u32[]{:S(2)}) copy-start(f32[4]{0:T(128)} %param.34) | copy-start | bytes 52
  159.3 38.9 %copy-start.3 = (bf16[256,256]{1,0:T(8,128)(2,1)S(1)}, bf16[256,256]{1,0:T(8,128)(2,1)}, u32[]{:S(2)}) copy-start(bf16[256,256]{1,0:T(8,128)(2,1)} %param.26) | copy-start | bytes 393220
  159.8 38.5 %copy-start.13 = (bf16[256,2048]{1,0:T(8,128)(2,1)S(1)}, bf16[256,2048]{1,0:T(8,128)(2,1)}, u32[]{:S(2)}) copy-start(bf16[256,2048]{1,0:T(8,128)(2,1)} %param.36) | copy-start | bytes 3145732
  199.8 31.8 %all-to-all-start = ((bf16[16,16,2048]{2,1,0:T(8,128)(2,1)}), bf16[16,16,2048]{2,1,0:T(8,128)(2,1)}, u32[]{:S(2)}, u32[]{:S(2)}) async-start(bf16[16,16,2048]{2,1,0:T(8,128)(2,1)} %bitcast.49), calls=%async_computation | async-start | bytes 2097152 | tf_op jit(solution)/shard_map/all_to_all | solution.py:64
  206.8 19.7 %reduce-scatter.7.cloned.1.call-start = ((), (), s32[]{:S(2)}) async-start(), calls=%async_computation.7 | async-start | bytes 589824
  210.7 30.4 %copy-start.9 = (f32[256,2]{0,1:T(2,128)S(1)}, f32[256,2]{0,1:T(2,128)}, u32[]{:S(2)}) copy-start(f32[256,2]{0,1:T(2,128)} %param.43) | copy-start | bytes 6148
  231.6 21.8 %all-to-all-start.3 = ((bf16[32,1,24,128]{3,2,1,0:T(8,128)(2,1)}), bf16[32,1,24,128]{3,2,1,0:T(8,128)(2,1)S(1)}, u32[]{:S(2)}, u32[]{:S(2)}) async-start(bf16[32,1,24,128]{3,2,1,0:T(8,128)(2,1)} %bitcast.73), calls=%async_computation.4 | async-start | bytes 393216 | tf_op jit(solution)/shard_map/all_to_all | solution.py:269
Sparse Core Ops, SparseCore 0:
  142.4 43.1 reduce-scatter.4
  215.1 11.4 reduce-scatter.6
